TPU v7x, 32 devices: a whole 2x2x4 slice. The times are simulated.
32 devices in a mesh: grp: 2 (over y), sp: 8 (over z, core), tp: 2 (over x).
Axes of the slice: x: 2, y: 2, z: 4, core: 2. Of those that a mesh axis runs over, the one named last changes fastest.
Arguments:
- query_plain: bfloat16 [2560, 1024], P(('grp', 'sp'), 'tp'), parts along dimension 0, may hold values from -6 to 6
- query_turn: bfloat16 [2560, 512], P(('grp', 'sp'), 'tp'), parts along dimension 0, may hold values from -40 to 40, as said below
- latent: bfloat16 [2560, 512], P(('grp', 'sp')), parts along dimension 0, may hold values from -6 to 6
- key_turn: bfloat16 [2560, 64], P(('grp', 'sp')), parts along dimension 0, may hold values from -40 to 40, as said below
- latent_norm_scale: bfloat16 [512], replicated, may hold values from 0.099609375 to 1.8984375
- plain_key_matrix: bfloat16 [512, 1024], P(None, 'tp'), may hold values from -0.25 to 0.25
- value_matrix: bfloat16 [512, 1024], P(None, 'tp'), may hold values from -0.25 to 0.25
- residual: bfloat16 [2560, 2048], P(('grp', 'sp', 'tp')), parts along dimension 0, may hold values from -6 to 6
- out_weight: bfloat16 [1024, 2048], replicated, may hold values from -6 to 6
- ffn_gain: bfloat16 [2048], replicated, may hold values from 0.099609375 to 1.8984375
- gate_weight: bfloat16 [8, 2048, 1024], P('sp', None, 'tp'), may hold values from -1 to 1
- up_weight: bfloat16 [8, 2048, 1024], P('sp', None, 'tp'), may hold values from -1 to 1
- down_weight: bfloat16 [8, 1024, 2048], P('sp', 'tp'), may hold values from -0.0625 to 0.0625
- routes: int32 [2560, 4], P(('grp', 'sp', 'tp')), parts along dimension 0, may hold values from 0 to 7, all different within a row; in each aligned block of 80 rows (0 to 79, 80 to 159, ...) at most 60 rows name the same one
- route_weights: float32 [2560, 4], P(('grp', 'sp', 'tp')), parts along dimension 0, may hold values from 0.1 to 0.6
Outputs:
- mixed: bfloat16 [2560, 2048], P(('grp', 'sp', 'tp')), parts along dimension 0
There are 2 independent parts, one for each index of `grp`. A program takes and returns all parts, laid end to end along the dimension named above; an argument that names none is the same for every part. Nothing has to cross between parts.
Inputs may be any that keep to these rules, and one draw needn't show every extreme that they name: `query_turn`: in the hidden draw some rows are large. `key_turn`: in the hidden draw some rows are large. `routes`: each row names 4 different experts. In each aligned block of 80 rows (the rows of one device) no expert is named more than 60 times, a bound that some block reaches.
All inputs are finite; a program needn't handle non-finite values.
Results may differ from a plain program's by a relative error of at most 0.015.
Values may be sent and summed in bfloat16 or wider, within the bound.
A program may use at most 128 MiB of HBM per device.

v0:
```python
import jax
import jax.numpy as jnp
from jax import lax
from jax.sharding import PartitionSpec as P

PLAIN_HEAD_WIDTH = 128
QK_ROPE = 64
VALUE_WIDTH = 128
GRID_W = 64
theta = 10000.0
eps = 1e-06
limit = 7.0
slope = 1.702


def turn(vector, row_shift, col_shift):
    width = vector.shape[-1]
    count = width // 4
    half = width // 2
    freqs = theta ** (-jnp.arange(count, dtype=jnp.float32) / count)
    extra = (1,) * (vector.ndim - 2)
    pieces = []
    for portion, shift in ((vector[..., :half], row_shift), (vector[..., half:], col_shift)):
        angle = (shift.astype(jnp.float32)[:, None] * freqs[None, :]).reshape(
            (shift.shape[0],) + extra + (count,)
        )
        lower = portion[..., :count]
        upper = portion[..., count:]
        pieces.append(
            jnp.concatenate(
                [
                    lower * jnp.cos(angle) - upper * jnp.sin(angle),
                    lower * jnp.sin(angle) + upper * jnp.cos(angle),
                ],
                axis=-1,
            )
        )
    return jnp.concatenate(pieces, axis=-1)


def norm_scale(values, gain):
    wide = values.astype(jnp.float32)
    return (
        wide
        * lax.rsqrt(jnp.mean(wide * wide, axis=-1, keepdims=True) + eps)
        * gain.astype(jnp.float32)
    )


def expert_active(rows, gate_w, up_w):
    gate_pre = jnp.minimum(jnp.dot(rows, gate_w, preferred_element_type=jnp.float32), limit)
    up_pre = jnp.clip(jnp.dot(rows, up_w, preferred_element_type=jnp.float32), -limit, limit)
    return ((up_pre + 1.0) * gate_pre * jax.nn.sigmoid(slope * gate_pre)).astype(jnp.bfloat16)


def expert_whole(rows, gate_w, up_w, down_w, groups):
    active = expert_active(rows, gate_w, up_w)
    piece = down_w.shape[0] // groups
    total = jnp.zeros((rows.shape[0], down_w.shape[1]), jnp.float32)
    for index in range(groups):
        product = jnp.dot(
            active[:, index * piece : (index + 1) * piece],
            down_w[index * piece : (index + 1) * piece],
            preferred_element_type=jnp.float32,
        )
        total = total + product.astype(jnp.bfloat16).astype(jnp.float32)
    return total.astype(jnp.bfloat16)


def on_device(
    query_plain,
    query_turn,
    latent,
    key_turn,
    latent_norm_scale,
    plain_key_matrix,
    value_matrix,
    residual,
    out_weight,
    ffn_gain,
    gate_weight,
    up_weight,
    down_weight,
    routes,
    route_weights,
):
    tok_dev = latent.shape[0]
    heads_dev = query_plain.shape[1] // PLAIN_HEAD_WIDTH
    model_width = residual.shape[1]
    place = lax.axis_index("sp") * tok_dev + jnp.arange(tok_dev, dtype=jnp.int32)
    grid_row = place // GRID_W
    grid_col = place % GRID_W
    normed_latent = norm_scale(latent, latent_norm_scale).astype(jnp.bfloat16)
    key_plain = jnp.dot(normed_latent, plain_key_matrix, preferred_element_type=jnp.float32).astype(
        jnp.bfloat16
    )
    values = jnp.dot(normed_latent, value_matrix, preferred_element_type=jnp.float32).astype(
        jnp.bfloat16
    )
    key_rot = turn(key_turn.astype(jnp.float32), grid_row, grid_col).astype(jnp.bfloat16)
    key_pairs = key_rot.reshape(tok_dev // 2, 2 * QK_ROPE)
    query_rot = turn(
        query_turn.astype(jnp.float32).reshape(tok_dev, heads_dev, QK_ROPE), grid_row, grid_col
    ).astype(jnp.bfloat16)
    plain_query = query_plain.reshape(tok_dev, heads_dev, PLAIN_HEAD_WIDTH)
    scale = (PLAIN_HEAD_WIDTH + QK_ROPE) ** (-0.5)
    most = jnp.full((heads_dev, tok_dev), -jnp.inf, jnp.float32)
    total = jnp.zeros((heads_dev, tok_dev), jnp.float32)
    summed = jnp.zeros((heads_dev, tok_dev, VALUE_WIDTH), jnp.float32)
    piece_keys = lax.all_gather(key_plain, "sp", axis=0, tiled=True)
    piece_values = lax.all_gather(values, "sp", axis=0, tiled=True)
    piece_pairs = lax.all_gather(key_pairs, "sp", axis=0, tiled=True)
    count = piece_keys.shape[0]
    piece_rot = piece_pairs.reshape(count, QK_ROPE)
    new_most = []
    new_total = []
    new_summed = []
    for head in range(heads_dev):
        head_keys = piece_keys[:, head * PLAIN_HEAD_WIDTH : (head + 1) * PLAIN_HEAD_WIDTH]
        head_values = piece_values[:, head * VALUE_WIDTH : (head + 1) * VALUE_WIDTH]
        scores = (
            jnp.einsum(
                "qd,kd->qk", plain_query[:, head], head_keys, preferred_element_type=jnp.float32
            )
            + jnp.einsum(
                "qd,kd->qk", query_rot[:, head], piece_rot, preferred_element_type=jnp.float32
            )
        ) * scale
        peak = jnp.max(scores, axis=1)
        factor = jnp.exp(most[head] - peak)
        weights = jnp.exp(scores - peak[:, None])
        new_total.append(total[head] * factor + jnp.sum(weights, axis=1))
        new_summed.append(
            summed[head] * factor[:, None]
            + jnp.dot(weights.astype(jnp.bfloat16), head_values, preferred_element_type=jnp.float32)
        )
        new_most.append(peak)
    total = jnp.stack(new_total)
    summed = jnp.stack(new_summed)
    attended = jnp.transpose((summed / total[..., None]).astype(jnp.bfloat16), (1, 0, 2)).reshape(
        tok_dev, heads_dev * VALUE_WIDTH
    )
    rows_dev = residual.shape[0]
    own_rows = lax.dynamic_slice_in_dim(
        out_weight, lax.axis_index("tp") * heads_dev * VALUE_WIDTH, heads_dev * VALUE_WIDTH, 0
    )
    projected = lax.psum_scatter(
        jnp.dot(attended, own_rows, preferred_element_type=jnp.float32).astype(jnp.bfloat16),
        "tp",
        scatter_dimension=0,
        tiled=True,
    ).astype(jnp.float32)
    hidden = (residual.astype(jnp.float32) + projected).astype(jnp.bfloat16)
    normed = norm_scale(hidden, ffn_gain).astype(jnp.bfloat16)
    top_count = routes.shape[1]
    experts_all = lax.axis_size("sp") * gate_weight.shape[0]
    capacity = min(rows_dev, max(2, rows_dev * top_count * 3 // (2 * experts_all)))
    flat_routes = routes.reshape(rows_dev * top_count)
    marks = (flat_routes[:, None] == jnp.arange(experts_all, dtype=jnp.int32)[None, :]).astype(
        jnp.int32
    )
    earlier = jnp.cumsum(marks, axis=0, dtype=jnp.int32) - marks
    slots = jnp.sum(earlier * marks, axis=1, dtype=jnp.int32)
    target = flat_routes * capacity + slots
    chosen = (
        target.reshape(rows_dev, top_count)[None, :, :]
        == jnp.arange(experts_all * capacity, dtype=jnp.int32)[:, None, None]
    )
    dispatch_table = jnp.sum(chosen.astype(jnp.bfloat16), axis=2)
    outgoing = jnp.dot(dispatch_table, normed, preferred_element_type=jnp.float32).astype(
        jnp.bfloat16
    )
    outgoing = outgoing.reshape(experts_all, capacity, model_width)
    gate_w = gate_weight[0]
    up_w = up_weight[0]
    down_w = down_weight[0]
    group = lax.axis_size("tp")
    gate_full, up_full, down_full = (
        lax.all_gather(gate_w, "tp", axis=1, tiled=True),
        lax.all_gather(up_w, "tp", axis=1, tiled=True),
        lax.all_gather(down_w, "tp", axis=0, tiled=True),
    )
    arrived = lax.all_to_all(outgoing, "sp", split_axis=0, concat_axis=0, tiled=True)
    result_rows = expert_whole(
        arrived.reshape(experts_all * capacity, model_width), gate_full, up_full, down_full, group
    )
    returned = lax.all_to_all(
        result_rows.reshape(experts_all, capacity, model_width),
        "sp",
        split_axis=0,
        concat_axis=0,
        tiled=True,
    )
    picked = returned.reshape(experts_all * capacity, model_width)[target]
    picked = picked.reshape(rows_dev, top_count, model_width).astype(jnp.float32)
    return (hidden.astype(jnp.float32) + jnp.sum(route_weights[..., None] * picked, axis=1)).astype(
        jnp.bfloat16
    )


def solution(mesh):
    placed = (
        P(("grp", "sp"), "tp"),
        P(("grp", "sp"), "tp"),
        P(("grp", "sp"), None),
        P(("grp", "sp"), None),
        P(),
        P(None, "tp"),
        P(None, "tp"),
        P(("grp", "sp", "tp"), None),
        P(),
        P(),
        P("sp", None, "tp"),
        P("sp", None, "tp"),
        P("sp", "tp", None),
        P(("grp", "sp", "tp"), None),
        P(("grp", "sp", "tp"), None),
    )
    return jax.shard_map(
        on_device,
        mesh=mesh,
        in_specs=placed,
        out_specs=P(("grp", "sp", "tp"), None),
        check_vma=False,
    )
```

profile of v0, /device:TPU:0, one launch (start us, length us, event | category | flops | bytes accessed | tf_op | source)
XLA Modules:
  0.0 335.4 jit_solution(11522728959038800007)
XLA Ops:
  6.6 1.1 fusion.38
  7.7 0.7 convert_element_type.119
  8.4 1.9 convolution_convert_fusion.5
  10.3 2.1 convolution_convert_fusion.4
  13.1 16.3 %all_gather.19 = bf16[640,128]{1,0:T(8,128)(2,1)S(1)} all-gather(bf16[80,128]{1,0:T(8,128)(2,1)S(1)} %convert_element_type.125), channel_id=1, replica_groups=mesh['grp'=2,'sp'=8,'tp'=2] {'sp'}, dimensions={0}, use_global_device_ids=true | all-gather | bytes 184320 | tf_op jit(solution)/shard_map/all_gather | solution.py:112
  30.0 7.3 %all-gather.9.cloned.1.call-done = bf16[1280,512]{1,0:T(8,128)(2,1)} async-done(((bf16[160,512]{1,0:T(8,128)(2,1)}), bf16[1280,512]{1,0:T(8,128)(2,1)}) %all-gather.9.cloned.1.call-update) | async-done | bytes 1310736 | tf_op jit(solution)/shard_map/all_gather | solution.py:110
  37.2 1.3 convolution_bitcast_fusion.3
  38.6 0.4 fusion.83
  39.0 0.3 convolution_bitcast_fusion.2
  39.3 0.4 fusion.82
  39.7 0.3 convolution_bitcast_fusion.1
  39.9 0.3 fusion.15
  40.5 0.4 fusion.81
  40.9 0.3 fusion.19
  41.2 0.3 convolution_bitcast_fusion
  41.4 0.4 fusion.80
  41.8 0.9 copy-done.1
  43.1 18.7 %all-gather.11.cloned.1.call-done = bf16[1280,512]{1,0:T(8,128)(2,1)} async-done(((bf16[160,512]{1,0:T(8,128)(2,1)}), bf16[1280,512]{1,0:T(8,128)(2,1)}) %all-gather.11.cloned.1.call-update) | async-done | bytes 1310736 | tf_op jit(solution)/shard_map/all_gather | solution.py:111
  61.8 1.4 fusion.14
  63.3 1.3 fusion.13
  64.6 0.3 fusion.12
  65.0 0.3 fusion.11
  65.3 3.0 convolution_convert_fusion.3
  68.4 0.5 all-gather.15.cloned.1.call-update
  69.0 0.5 all-gather.13.cloned.1.call-update
  69.8 0.9 reduce-window.6
  71.4 12.7 %reduce-scatter.2.cloned.1.call-done = bf16[80,2048]{1,0:T(8,128)(2,1)} async-done(((bf16[160,2048]{1,0:T(8,128)(2,1)}), bf16[80,2048]{1,0:T(8,128)(2,1)}) %reduce-scatter.2.cloned.1.call-update) | async-done | bytes 327696 | tf_op jit(solution)/shard_map/reduce_scatter | solution.py:147
  84.1 1.2 fusion.23
  85.3 1.7 convolution_convert_fusion.2
  87.0 1.6 reshape.371
  88.6 4.6 %all-to-all-start = ((bf16[8,60,2048]{2,1,0:T(8,128)(2,1)}), bf16[8,60,2048]{2,1,0:T(8,128)(2,1)S(1)}, u32[]{:S(2)}, u32[]{:S(2)}) async-start(bf16[8,60,2048]{2,1,0:T(8,128)(2,1)} %reshape.371), calls=%async_computation.1 | async-start | bytes 4194304 | tf_op jit(solution)/shard_map/all_to_all | solution.py:183
  93.4 0.3 all-gather.17.cloned.1.call-update
  93.8 48.5 %all-to-all-done = bf16[8,60,2048]{2,1,0:T(8,128)(2,1)S(1)} async-done(((bf16[8,60,2048]{2,1,0:T(8,128)(2,1)}), bf16[8,60,2048]{2,1,0:T(8,128)(2,1)S(1)}, u32[]{:S(2)}, u32[]{:S(2)}) %all-to-all-start) | async-done | bytes 1966112 | tf_op jit(solution)/shard_map/all_to_all | solution.py:183
  142.2 1.5 reshape.372
  143.7 6.4 %fusion = f32[480,1024]{1,0:T(8,128)} fusion(bf16[480,2048]{1,0:T(8,128)(2,1)} %reshape.372, bf16[1,2048,1024]{2,1,0:T(8,128)(2,1)} %all-gather.15.cloned.1.call-done), kind=kOutput, calls=%fused_computation.1 | convolution fusion | flops 2013265920 | bytes 8126464 | tf_op jit(solution)/shard_map/dot_general | solution.py:51
  150.1 50.3 %all-gather.13.cloned.1.call-done = bf16[1,2048,1024]{2,1,0:T(8,128)(2,1)} async-done(((bf16[1,2048,512]{2,1,0:T(8,128)(2,1)}), bf16[1,2048,1024]{2,1,0:T(8,128)(2,1)}) %all-gather.13.cloned.1.call-update) | async-done | bytes 4194320 | tf_op jit(solution)/shard_map/all_gather | solution.py:180
  200.4 6.5 %multiply_convert_fusion = bf16[480,1024]{1,0:T(8,128)(2,1)} fusion(f32[480,1024]{1,0:T(8,128)} %fusion, bf16[480,2048]{1,0:T(8,128)(2,1)S(1)} %copy-done.5, bf16[1,2048,1024]{2,1,0:T(8,128)(2,1)} %all-gather.13.cloned.1.call-done), kind=kOutput, calls=%fused_computation.26 | convolution fusion | flops 2018181120 | bytes 9109504 | tf_op jit(solution)/shard_map/dot_general | solution.py:52
  206.9 51.7 %all-gather.17.cloned.1.call-done = bf16[1,1024,2048]{2,1,0:T(8,128)(2,1)} async-done(((bf16[1,512,2048]{2,1,0:T(8,128)(2,1)}), bf16[1,1024,2048]{2,1,0:T(8,128)(2,1)}) %all-gather.17.cloned.1.call-update) | async-done | bytes 4194320 | tf_op jit(solution)/shard_map/all_gather | solution.py:181
  258.6 3.1 convolution_convert_fusion
  261.8 1.2 add_convert_fusion
  263.0 1.5 reshape.373
  264.5 4.7 %all-to-all-start.1 = ((bf16[8,60,2048]{2,1,0:T(8,128)(2,1)}), bf16[8,60,2048]{2,1,0:T(8,128)(2,1)}, u32[]{:S(2)}, u32[]{:S(2)}) async-start(bf16[8,60,2048]{2,1,0:T(8,128)(2,1)} %reshape.373), calls=%async_computation.2 | async-start | bytes 4194304 | tf_op jit(solution)/shard_map/all_to_all | solution.py:187
  269.5 48.9 %all-to-all-done.1 = bf16[8,60,2048]{2,1,0:T(8,128)(2,1)} async-done(((bf16[8,60,2048]{2,1,0:T(8,128)(2,1)}), bf16[8,60,2048]{2,1,0:T(8,128)(2,1)}, u32[]{:S(2)}, u32[]{:S(2)}) %all-to-all-start.1) | async-done | bytes 1966112 | tf_op jit(solution)/shard_map/all_to_all | solution.py:187
  318.4 1.7 reshape.374
  320.1 3.0 gather_fusion
  323.2 2.6 reshape.378
  325.8 1.9 multiply_reduce_fusion
  327.7 0.8 fusion.26
  (81 shorter events, 3.5 us)
Async XLA Ops:
  6.5 1.9 copy-start
  6.5 6.0 %copy-start.10 = (bf16[160,64]{0,1:T(8,128)(2,1)S(1)}, bf16[160,64]{0,1:T(8,128)(2,1)}, u32[]{:S(2)}) copy-start(bf16[160,64]{0,1:T(8,128)(2,1)} %param.18) | copy-start | bytes 61444
  6.5 6.0 %copy-start.9 = (bf16[160,256]{1,0:T(8,128)(2,1)S(1)}, bf16[160,256]{1,0:T(8,128)(2,1)}, u32[]{:S(2)}) copy-start(bf16[160,256]{1,0:T(8,128)(2,1)} %param.16) | copy-start | bytes 245764
  6.5 23.0 %copy-start.8 = (bf16[160,512]{1,0:T(8,128)(2,1)S(1)}, bf16[160,512]{1,0:T(8,128)(2,1)}, u32[]{:S(2)}) copy-start(bf16[160,512]{1,0:T(8,128)(2,1)} %param.15) | copy-start | bytes 491524
  6.5 30.7 %all-gather.9.cloned.1.call-start = ((), (), s32[]{:S(2)}) async-start(), calls=%async_computation.3 | async-start | bytes 1474560 | tf_op jit(solution)/shard_map/all_gather | solution.py:110
  10.3 51.6 %all-gather.11.cloned.1.call-start = ((), (), s32[]{:S(2)}) async-start(), calls=%async_computation.4 | async-start | bytes 1474560 | tf_op jit(solution)/shard_map/all_gather | solution.py:111
  12.4 71.7 %reduce-scatter.2.cloned.1.call-start = ((), (), s32[]{:S(2)}) async-start(), calls=%async_computation.5 | async-start | bytes 983040 | tf_op jit(solution)/shard_map/reduce_scatter | solution.py:147
  37.2 1.8 copy-start.6
  41.8 0.9 copy-start.1
  61.8 2.8 copy-start.7
  61.8 3.1 copy-start.2
  68.3 1.2 copy-start.12
  68.3 2.9 copy-start.11
  68.4 15.7 %copy-start.3 = (bf16[80,2048]{1,0:T(8,128)(2,1)S(1)}, bf16[80,2048]{1,0:T(8,128)(2,1)}, u32[]{:S(2)}) copy-start(bf16[80,2048]{1,0:T(8,128)(2,1)} %param.22) | copy-start | bytes 983044
  68.4 75.3 %all-gather.15.cloned.1.call-start = ((), (), s32[]{:S(2)}) async-start(), calls=%async_computation.7 | async-start | bytes 6291456 | tf_op jit(solution)/shard_map/all_gather | solution.py:179
  68.9 131.5 %all-gather.13.cloned.1.call-start = ((), (), s32[]{:S(2)}) async-start(), calls=%async_computation.6 | async-start | bytes 6291456 | tf_op jit(solution)/shard_map/all_gather | solution.py:180
  88.6 53.6 %all-to-all-start = ((bf16[8,60,2048]{2,1,0:T(8,128)(2,1)}), bf16[8,60,2048]{2,1,0:T(8,128)(2,1)S(1)}, u32[]{:S(2)}, u32[]{:S(2)}) async-start(bf16[8,60,2048]{2,1,0:T(8,128)(2,1)} %reshape.371), calls=%async_computation.1 | async-start | bytes 4194304 | tf_op jit(solution)/shard_map/all_to_all | solution.py:183
  93.2 165.4 %all-gather.17.cloned.1.call-start = ((), (), s32[]{:S(2)}) async-start(), calls=%async_computation.8 | async-start | bytes 6291456 | tf_op jit(solution)/shard_map/all_gather | solution.py:181
  143.7 56.7 %copy-start.5 = (bf16[480,2048]{1,0:T(8,128)(2,1)S(1)}, bf16[480,2048]{1,0:T(8,128)(2,1)}, u32[]{:S(2)}) copy-start(bf16[480,2048]{1,0:T(8,128)(2,1)} %reshape.372) | copy-start | bytes 5898244
  258.6 3.1 copy-start.14
  258.6 3.2 copy-start.15
  264.5 4.8 %copy-start.13 = (f32[80,4]{0,1:T(4,128)S(1)}, f32[80,4]{0,1:T(4,128)}, u32[]{:S(2)}) copy-start(f32[80,4]{0,1:T(4,128)} %param.29) | copy-start | bytes 3844
  264.5 53.9 %all-to-all-start.1 = ((bf16[8,60,2048]{2,1,0:T(8,128)(2,1)}), bf16[8,60,2048]{2,1,0:T(8,128)(2,1)}, u32[]{:S(2)}, u32[]{:S(2)}) async-start(bf16[8,60,2048]{2,1,0:T(8,128)(2,1)} %reshape.373), calls=%async_computation.2 | async-start | bytes 4194304 | tf_op jit(solution)/shard_map/all_to_all | solution.py:187
  325.8 1.9 copy-start.4
Sparse Core Ops, SparseCore 0:
  10.4 26.7 all-gather.8
  38.9 22.9 all-gather.10
  68.5 15.5 reduce-scatter.1
  85.5 56.7 all-gather.14
  143.6 56.7 all-gather.12
  201.8 56.7 all-gather.16
where the time goes:
time: 336 us; the launch traced here: 335 us
  waiting for transfers between devices  239 us (71%)
  matrix products  33 us (10%)
  blocking collectives  16.3 us (5%)
  local copies, waits for them, and re-layouts  14.6 us (4%)
  between operations  13.9 us (4%)
  starting transfers between devices  9.75 us (3%)
  other arithmetic  8.39 us (2%)
    all_gather x1, waiting for transfers between devices, on_device(): lax.all_gather(down_w, 'tp', axis=0, tiled=True)  51.7 us
    all_gather x1, waiting for transfers between devices, on_device(): lax.all_gather(up_w, 'tp', axis=1, tiled=True)  50.3 us
    all_to_all x1, waiting for transfers between devices, on_device(): lax.all_to_all(result_rows.reshape(experts_all, capacity, model_width), '...  48.9 us
    all_to_all x1, waiting for transfers between devices, on_device(): lax.all_to_all(outgoing, 'sp', split_axis=0, concat_axis=0, tiled=True)  48.5 us
    all_gather x1, waiting for transfers between devices, on_device(): piece_values = lax.all_gather(values, 'sp', axis=0, tiled=True)  18.7 us
    all_gather x1, blocking collectives, on_device(): piece_pairs = lax.all_gather(key_pairs, 'sp', axis=0, tiled=True)  16.3 us
    reduce_scatter x1, waiting for transfers between devices, on_device(): lax.psum_scatter(jnp.dot(attended, own_rows, preferred_element_type=jnp.f...  12.7 us
    all_gather x1, waiting for transfers between devices, on_device(): piece_keys = lax.all_gather(key_plain, 'sp', axis=0, tiled=True)  7.27 us
  transfers between devices with their start and end apart: 8, of which 7 were waited for; matrix products, arithmetic and copies ran while one was open for 9% of the time, Pallas kernels for 0%

commit v1 on v0

--- a/solution.py
+++ b/solution.py
@@ -178,7 +178,9 @@
     gate_full, up_full, down_full = (
         lax.all_gather(gate_w, "tp", axis=1, tiled=True),
         lax.all_gather(up_w, "tp", axis=1, tiled=True),
-        lax.all_gather(down_w, "tp", axis=0, tiled=True),
+        jnp.concatenate(
+            lax.all_to_all(jnp.stack([down_w] * lax.axis_size("tp")), "tp", 0, 0), axis=0
+        ),
     )
     arrived = lax.all_to_all(outgoing, "sp", split_axis=0, concat_axis=0, tiled=True)
     result_rows = expert_whole(

time: 336 us -> 325 us (0.967)
  waiting for transfers between devices: 239 us -> 216 us
  starting transfers between devices: 9.75 us -> 15.1 us
  other arithmetic: 8.39 us -> 13.4 us
    all_gather x1 -> x0, waiting for transfers between devices: 51.7 us -> none  [on_device(): lax.all_gather(down_w, 'tp', axis=0, tiled=True)]
    all_gather x1, waiting for transfers between devices: 50.3 us -> 83.5 us  [on_device(): lax.all_gather(up_w, 'tp', axis=1, tiled=True)]
    all_to_all x0 -> x1, starting transfers between devices: none -> 5.8 us  [on_device(): lax.all_to_all(jnp.stack([down_w] * lax.axis_size('tp')), 'tp', 0, 0)]
    all_to_all x1, waiting for transfers between devices: 48.5 us -> 43.5 us  [on_device(): lax.all_to_all(outgoing, 'sp', split_axis=0, concat_axis=0, tiled=True)]
    another operation x5 -> x6, other arithmetic: 1.03 us -> 5.99 us  [the longest x1 4.96 us: on_device(): jnp.stack([down_w] * lax.axis_size('tp'))]
  transfers between devices with their start and end apart: 8 -> 8, of which waited for: 7 -> 6; matrix products, arithmetic and copies ran while one was open for 9% -> 11% of each run, Pallas kernels for 0% -> 0%
where the time goes in v1:
time: 325 us; the launch traced here: 324 us
  waiting for transfers between devices  216 us (66%)
  matrix products  35.4 us (11%)
  blocking collectives  16.3 us (5%)
  starting transfers between devices  15.1 us (5%)
  local copies, waits for them, and re-layouts  14.6 us (4%)
  between operations  13.6 us (4%)
  other arithmetic  13.4 us (4%)
    all_gather x1, waiting for transfers between devices, on_device(): lax.all_gather(up_w, 'tp', axis=1, tiled=True)  83.5 us
    all_to_all x1, waiting for transfers between devices, on_device(): lax.all_to_all(result_rows.reshape(experts_all, capacity, model_width), '...  48.8 us
    all_to_all x1, waiting for transfers between devices, on_device(): lax.all_to_all(outgoing, 'sp', split_axis=0, concat_axis=0, tiled=True)  43.5 us
    all_gather x1, waiting for transfers between devices, on_device(): piece_values = lax.all_gather(values, 'sp', axis=0, tiled=True)  18.7 us
    all_gather x1, blocking collectives, on_device(): piece_pairs = lax.all_gather(key_pairs, 'sp', axis=0, tiled=True)  16.3 us
    reduce_scatter x1, waiting for transfers between devices, on_device(): lax.psum_scatter(jnp.dot(attended, own_rows, preferred_element_type=jnp.f...  13.3 us
    all_gather x1, waiting for transfers between devices, on_device(): piece_keys = lax.all_gather(key_plain, 'sp', axis=0, tiled=True)  7.27 us
    dot_general x1, matrix products, expert_active(): jnp.dot(rows, gate_w, preferred_element_type=jnp.float32)  7.26 us
  transfers between devices with their start and end apart: 8, of which 6 were waited for; matrix products, arithmetic and copies ran while one was open for 11% of the time, Pallas kernels for 0%

profile of v1, /device:TPU:0, one launch (start us, length us, event | category | flops | bytes accessed | tf_op | source)
XLA Modules:
  0.0 324.4 jit_solution(773207930126809901)
XLA Ops:
  6.6 1.1 fusion.38
  7.7 0.7 convert_element_type.119
  8.4 1.9 convolution_convert_fusion.5
  10.3 2.1 convolution_convert_fusion.4
  13.1 16.3 %all_gather.16 = bf16[640,128]{1,0:T(8,128)(2,1)S(1)} all-gather(bf16[80,128]{1,0:T(8,128)(2,1)S(1)} %convert_element_type.125), channel_id=1, replica_groups=mesh['grp'=2,'sp'=8,'tp'=2] {'sp'}, dimensions={0}, use_global_device_ids=true | all-gather | bytes 184320 | tf_op jit(solution)/shard_map/all_gather | solution.py:112
  30.0 7.3 %all-gather.7.cloned.1.call-done = bf16[1280,512]{1,0:T(8,128)(2,1)} async-done(((bf16[160,512]{1,0:T(8,128)(2,1)}), bf16[1280,512]{1,0:T(8,128)(2,1)}) %all-gather.7.cloned.1.call-update) | async-done | bytes 1310736 | tf_op jit(solution)/shard_map/all_gather | solution.py:110
  37.2 1.3 convolution_bitcast_fusion.3
  38.6 0.4 fusion.83
  39.0 0.3 convolution_bitcast_fusion.2
  39.3 0.4 fusion.82
  39.7 0.3 convolution_bitcast_fusion.1
  39.9 0.3 fusion.15
  40.5 0.4 fusion.81
  40.9 0.3 fusion.19
  41.2 0.3 convolution_bitcast_fusion
  41.4 0.4 fusion.80
  41.8 0.9 copy-done.2
  43.1 18.7 %all-gather.9.cloned.1.call-done = bf16[1280,512]{1,0:T(8,128)(2,1)} async-done(((bf16[160,512]{1,0:T(8,128)(2,1)}), bf16[1280,512]{1,0:T(8,128)(2,1)}) %all-gather.9.cloned.1.call-update) | async-done | bytes 1310736 | tf_op jit(solution)/shard_map/all_gather | solution.py:111
  61.8 1.4 fusion.14
  63.3 1.3 fusion.13
  64.6 0.3 fusion.12
  65.0 0.3 fusion.11
  65.3 3.0 convolution_convert_fusion.3
  68.4 0.5 all-gather.13.cloned.1.call-update
  69.2 0.9 reduce-window.6
  70.8 13.3 %reduce-scatter.2.cloned.1.call-done = bf16[80,2048]{1,0:T(8,128)(2,1)} async-done(((bf16[160,2048]{1,0:T(8,128)(2,1)}), bf16[80,2048]{1,0:T(8,128)(2,1)}) %reduce-scatter.2.cloned.1.call-update) | async-done | bytes 327696 | tf_op jit(solution)/shard_map/reduce_scatter | solution.py:147
  84.1 1.2 fusion.23
  85.3 1.7 convolution_convert_fusion.2
  87.0 1.6 reshape.374
  88.6 4.6 %all-to-all-start = ((bf16[8,60,2048]{2,1,0:T(8,128)(2,1)}), bf16[8,60,2048]{2,1,0:T(8,128)(2,1)S(1)}, u32[]{:S(2)}, u32[]{:S(2)}) async-start(bf16[8,60,2048]{2,1,0:T(8,128)(2,1)} %reshape.374), calls=%async_computation.1 | async-start | bytes 4194304 | tf_op jit(solution)/shard_map/all_to_all | solution.py:185
  93.2 0.5 all-gather.11.cloned.1.call-update
  93.8 5.0 %pad_maximum_fusion = bf16[2,512,2048]{2,1,0:T(8,128)(2,1)} fusion(bf16[1,512,2048]{2,1,0:T(8,128)(2,1)} %param.27), kind=kLoop, calls=%fused_computation.1 | loop fusion | flops 2097152 | bytes 6291456 | tf_op jit(solution)/shard_map/stack | solution.py:182
  98.7 43.5 %all-to-all-done = bf16[8,60,2048]{2,1,0:T(8,128)(2,1)S(1)} async-done(((bf16[8,60,2048]{2,1,0:T(8,128)(2,1)}), bf16[8,60,2048]{2,1,0:T(8,128)(2,1)S(1)}, u32[]{:S(2)}, u32[]{:S(2)}) %all-to-all-start) | async-done | bytes 1966112 | tf_op jit(solution)/shard_map/all_to_all | solution.py:185
  142.2 5.8 %all-to-all-start.1 = ((bf16[2,512,2048]{2,1,0:T(8,128)(2,1)}), bf16[2,512,2048]{2,1,0:T(8,128)(2,1)}, u32[]{:S(2)}, u32[]{:S(2)}) async-start(bf16[2,512,2048]{2,1,0:T(8,128)(2,1)} %pad_maximum_fusion), calls=%async_computation.2 | async-start | bytes 8388608 | tf_op jit(solution)/shard_map/all_to_all | solution.py:182
  148.0 1.5 reshape.375
  149.5 7.3 %fusion = f32[480,1024]{1,0:T(8,128)} fusion(bf16[480,2048]{1,0:T(8,128)(2,1)} %reshape.375, bf16[1,2048,1024]{2,1,0:T(8,128)(2,1)} %all-gather.13.cloned.1.call-done), kind=kOutput, calls=%fused_computation.2 | convolution fusion | flops 2013265920 | bytes 8126464 | tf_op jit(solution)/shard_map/dot_general | solution.py:51
  156.8 83.5 %all-gather.11.cloned.1.call-done = bf16[1,2048,1024]{2,1,0:T(8,128)(2,1)} async-done(((bf16[1,2048,512]{2,1,0:T(8,128)(2,1)}), bf16[1,2048,1024]{2,1,0:T(8,128)(2,1)}) %all-gather.11.cloned.1.call-update) | async-done | bytes 4194320 | tf_op jit(solution)/shard_map/all_gather | solution.py:180
  240.3 6.4 %multiply_convert_fusion = bf16[480,1024]{1,0:T(8,128)(2,1)} fusion(f32[480,1024]{1,0:T(8,128)} %fusion, bf16[480,2048]{1,0:T(8,128)(2,1)S(1)} %copy-done.6, bf16[1,2048,1024]{2,1,0:T(8,128)(2,1)} %all-gather.11.cloned.1.call-done), kind=kOutput, calls=%fused_computation.27 | convolution fusion | flops 2018181120 | bytes 9109504 | tf_op jit(solution)/shard_map/dot_general | solution.py:52
  246.7 3.0 convolution_convert_fusion
  249.8 2.8 add_convert_fusion
  252.6 1.5 reshape.376
  254.1 4.5 %all-to-all-start.2 = ((bf16[8,60,2048]{2,1,0:T(8,128)(2,1)}), bf16[8,60,2048]{2,1,0:T(8,128)(2,1)}, u32[]{:S(2)}, u32[]{:S(2)}) async-start(bf16[8,60,2048]{2,1,0:T(8,128)(2,1)} %reshape.376), calls=%async_computation.3 | async-start | bytes 4194304 | tf_op jit(solution)/shard_map/all_to_all | solution.py:189
  258.8 48.8 %all-to-all-done.2 = bf16[8,60,2048]{2,1,0:T(8,128)(2,1)} async-done(((bf16[8,60,2048]{2,1,0:T(8,128)(2,1)}), bf16[8,60,2048]{2,1,0:T(8,128)(2,1)}, u32[]{:S(2)}, u32[]{:S(2)}) %all-to-all-start.2) | async-done | bytes 1966112 | tf_op jit(solution)/shard_map/all_to_all | solution.py:189
  307.6 1.7 reshape.377
  309.4 3.0 gather_fusion
  312.4 2.7 reshape.381
  315.1 1.9 multiply_reduce_fusion
  317.0 0.8 fusion.26
  (81 shorter events, 3.2 us)
Async XLA Ops:
  6.5 1.9 copy-start
  6.5 6.0 %copy-start.11 = (bf16[160,64]{0,1:T(8,128)(2,1)S(1)}, bf16[160,64]{0,1:T(8,128)(2,1)}, u32[]{:S(2)}) copy-start(bf16[160,64]{0,1:T(8,128)(2,1)} %param.18) | copy-start | bytes 61444
  6.5 6.0 %copy-start.10 = (bf16[160,256]{1,0:T(8,128)(2,1)S(1)}, bf16[160,256]{1,0:T(8,128)(2,1)}, u32[]{:S(2)}) copy-start(bf16[160,256]{1,0:T(8,128)(2,1)} %param.16) | copy-start | bytes 245764
  6.5 23.0 %copy-start.9 = (bf16[160,512]{1,0:T(8,128)(2,1)S(1)}, bf16[160,512]{1,0:T(8,128)(2,1)}, u32[]{:S(2)}) copy-start(bf16[160,512]{1,0:T(8,128)(2,1)} %param.15) | copy-start | bytes 491524
  6.5 30.7 %all-gather.7.cloned.1.call-start = ((), (), s32[]{:S(2)}) async-start(), calls=%async_computation.4 | async-start | bytes 1474560 | tf_op jit(solution)/shard_map/all_gather | solution.py:110
  10.3 51.6 %all-gather.9.cloned.1.call-start = ((), (), s32[]{:S(2)}) async-start(), calls=%async_computation.5 | async-start | bytes 1474560 | tf_op jit(solution)/shard_map/all_gather | solution.py:111
  12.4 71.7 %reduce-scatter.2.cloned.1.call-start = ((), (), s32[]{:S(2)}) async-start(), calls=%async_computation.6 | async-start | bytes 983040 | tf_op jit(solution)/shard_map/reduce_scatter | solution.py:147
  37.2 1.8 copy-start.7
  41.8 0.9 copy-start.2
  61.8 2.8 copy-start.8
  61.8 3.1 copy-start.3
  68.3 0.7 copy-start.13
  68.3 2.3 copy-start.12
  68.3 15.8 %copy-start.4 = (bf16[80,2048]{1,0:T(8,128)(2,1)S(1)}, bf16[80,2048]{1,0:T(8,128)(2,1)}, u32[]{:S(2)}) copy-start(bf16[80,2048]{1,0:T(8,128)(2,1)} %param.22) | copy-start | bytes 983044
  68.3 81.2 %all-gather.13.cloned.1.call-start = ((), (), s32[]{:S(2)}) async-start(), calls=%async_computation.8 | async-start | bytes 6291456 | tf_op jit(solution)/shard_map/all_gather | solution.py:179
  88.6 53.6 %all-to-all-start = ((bf16[8,60,2048]{2,1,0:T(8,128)(2,1)}), bf16[8,60,2048]{2,1,0:T(8,128)(2,1)S(1)}, u32[]{:S(2)}, u32[]{:S(2)}) async-start(bf16[8,60,2048]{2,1,0:T(8,128)(2,1)} %reshape.374), calls=%async_computation.1 | async-start | bytes 4194304 | tf_op jit(solution)/shard_map/all_to_all | solution.py:185
  93.2 147.1 %all-gather.11.cloned.1.call-start = ((), (), s32[]{:S(2)}) async-start(), calls=%async_computation.7 | async-start | bytes 6291456 | tf_op jit(solution)/shard_map/all_gather | solution.py:180
  142.2 104.5 %all-to-all-start.1 = ((bf16[2,512,2048]{2,1,0:T(8,128)(2,1)}), bf16[2,512,2048]{2,1,0:T(8,128)(2,1)}, u32[]{:S(2)}, u32[]{:S(2)}) async-start(bf16[2,512,2048]{2,1,0:T(8,128)(2,1)} %pad_maximum_fusion), calls=%async_computation.2 | async-start | bytes 8388608 | tf_op jit(solution)/shard_map/all_to_all | solution.py:182
  149.5 90.8 %copy-start.6 = (bf16[480,2048]{1,0:T(8,128)(2,1)S(1)}, bf16[480,2048]{1,0:T(8,128)(2,1)}, u32[]{:S(2)}) copy-start(bf16[480,2048]{1,0:T(8,128)(2,1)} %reshape.375) | copy-start | bytes 5898244
  246.7 3.0 copy-start.15
  254.1 4.6 %copy-start.14 = (f32[80,4]{0,1:T(4,128)S(1)}, f32[80,4]{0,1:T(4,128)}, u32[]{:S(2)}) copy-start(f32[80,4]{0,1:T(4,128)} %param.29) | copy-start | bytes 3844
  254.1 53.5 %all-to-all-start.2 = ((bf16[8,60,2048]{2,1,0:T(8,128)(2,1)}), bf16[8,60,2048]{2,1,0:T(8,128)(2,1)}, u32[]{:S(2)}, u32[]{:S(2)}) async-start(bf16[8,60,2048]{2,1,0:T(8,128)(2,1)} %reshape.376), calls=%async_computation.3 | async-start | bytes 4194304 | tf_op jit(solution)/shard_map/all_to_all | solution.py:189
  312.4 5.5 %copy-start.1 = (bf16[512,512]{1,0:T(8,128)(2,1)S(1)}, bf16[512,512]{1,0:T(8,128)(2,1)}, u32[]{:S(2)}) copy-start(bf16[512,512]{1,0:T(8,128)(2,1)} %param.20) | copy-start | bytes 1572868
  315.1 1.9 copy-start.5
Sparse Core Ops, SparseCore 0:
  10.4 26.7 all-gather.6
  38.9 22.9 all-gather.8
  68.4 15.5 reduce-scatter.1
  85.5 56.7 all-gather.12
  143.6 96.5 all-gather.10
